TPU v7x, 32 devices: a whole 2x2x4 slice. The times are simulated.
32 devices in a mesh: ra: 4 (over z), cb: 4 (over y, x), dp: 2 (over core).
Axes of the slice: x: 2, y: 2, z: 4, core: 2. Of those that a mesh axis runs over, the one named last changes fastest.
Arguments:
- tokens: bfloat16 [1024, 4096], P('dp', 'ra'), may hold values from -160 to 160, as said below
- first_gain: bfloat16 [4096], P('ra'), may hold values from 0.099609375 to 1.8984375
- first_gate: bfloat16 [4096, 6144], P('ra', 'cb'), may hold values from -0.125 to 0.125
- first_up: bfloat16 [4096, 6144], P('ra', 'cb'), may hold values from -0.125 to 0.125
- first_down: bfloat16 [6144, 4096], P(('cb', 'ra')), may hold values from -0.109375 to 0.109375
- first_branch: bfloat16 [4096], P('ra'), may hold values from 1 to 4
- second_gain: bfloat16 [4096], P('ra'), may hold values from 0.099609375 to 1.8984375
- second_gate: bfloat16 [4096, 6144], P('ra', 'cb'), may hold values from -0.125 to 0.125
- second_up: bfloat16 [4096, 6144], P('ra', 'cb'), may hold values from -0.125 to 0.125
- second_down: bfloat16 [6144, 4096], P(('cb', 'ra')), may hold values from -0.109375 to 0.109375
- second_branch: bfloat16 [4096], P('ra'), may hold values from 1 to 4
Outputs:
- mixed_out: bfloat16 [1024, 4096], P('dp', 'ra')
Inputs may be any that keep to these rules, and one draw needn't show every extreme that they name: `tokens`: activations whose scale varies by token and by feature.
All inputs are finite; a program needn't handle non-finite values.
Results may differ from a plain program's by a relative error of at most 0.035.
Values may be sent and summed in bfloat16 or wider, within the bound.
A program may use at most 64 MiB of HBM per device.

v0:
```python
import jax
import jax.numpy as jnp
from jax import lax
from jax.sharding import PartitionSpec as P

epsilon = 1e-06
residual_scale = 0.25


def half_step(values, norm_gain, w_gate, w_up, w_down, branch_gain):
    wide_values = values.astype(jnp.float32)
    width = values.shape[1] * lax.axis_size("ra")
    squares = lax.psum(jnp.sum(wide_values * wide_values, axis=1), "ra")
    scale = lax.rsqrt(squares / width + epsilon)
    normed = (wide_values * scale[:, None] * norm_gain.astype(jnp.float32)).astype(jnp.bfloat16)
    gate_part = jnp.dot(normed, w_gate, preferred_element_type=jnp.float32)
    up_part = jnp.dot(normed, w_up, preferred_element_type=jnp.float32)
    gate, upward = (
        lax.psum_scatter(
            gate_part.astype(jnp.bfloat16), "ra", scatter_dimension=1, tiled=True
        ).astype(jnp.float32),
        lax.psum_scatter(
            up_part.astype(jnp.bfloat16), "ra", scatter_dimension=1, tiled=True
        ).astype(jnp.float32),
    )
    hidden = (jax.nn.silu(gate) * upward).astype(jnp.bfloat16)
    terms = jnp.dot(hidden, w_down, preferred_element_type=jnp.float32)
    partial_value = lax.psum_scatter(
        terms.astype(jnp.bfloat16), "ra", scatter_dimension=1, tiled=True
    )
    branch = lax.psum(partial_value, "cb").astype(jnp.float32)
    return (residual_scale * wide_values + 0.5 * branch_gain.astype(jnp.float32) * branch).astype(
        jnp.bfloat16
    )


def shards(
    tokens,
    first_gain,
    first_gate,
    first_up,
    first_down,
    first_branch,
    second_gain,
    second_gate,
    second_up,
    second_down,
    second_branch,
):
    middle = half_step(tokens, first_gain, first_gate, first_up, first_down, first_branch)
    return half_step(middle, second_gain, second_gate, second_up, second_down, second_branch)


def solution(mesh):
    return jax.shard_map(
        shards,
        mesh=mesh,
        in_specs=(
            P("dp", "ra"),
            P("ra"),
            P("ra", "cb"),
            P("ra", "cb"),
            P(("cb", "ra"), None),
            P("ra"),
            P("ra"),
            P("ra", "cb"),
            P("ra", "cb"),
            P(("cb", "ra"), None),
            P("ra"),
        ),
        out_specs=P("dp", "ra"),
        check_vma=False,
    )
```

profile of v0, /device:TPU:0, one launch (start us, length us, event | category | flops | bytes accessed | tf_op | source)
XLA Modules:
  0.0 481.5 jit_solution(15496341558290964854)
XLA Ops:
  6.5 0.0 copy-start
  6.5 0.0 reduce-scatter.19.cloned.1.call-start
  6.5 1.7 fusion.2
  8.2 13.5 %psum.28 = f32[512]{0:T(512)S(1)} all-reduce(f32[512]{0:T(512)S(1)} %fusion.2), channel_id=1, replica_groups=mesh['ra'=4,'cb'=4,'dp'=2] {'ra'}, use_global_device_ids=true, to_apply=%region_1.0 | all-reduce | flops 512 | bytes 4096 | tf_op jit(solution)/shard_map/psum | solution.py:13
  21.7 0.7 convert_element_type.74
  22.4 5.3 %convolution_convert_fusion.5 = bf16[512,1536]{1,0:T(8,128)(2,1)} fusion(bf16[1024,1536]{1,0:T(8,128)(2,1)} %param.13, bf16[512,1024]{1,0:T(8,128)(2,1)} %param.11, f32[1024]{0:T(1024)S(1)} %convert_element_type.74, f32[512]{0:T(512)S(1)} %add_rsqrt_fusion.1), kind=kOutput, calls=%fused_computation.11 | convolution fusion | flops 1613496320 | bytes 5773312 | tf_op jit(solution)/shard_map/dot_general | solution.py:16
  27.6 2.6 copy.12
  30.2 0.0 reduce-scatter.19.cloned.1.call-update
  30.3 0.0 reduce-scatter.21.cloned.1.call-start
  30.3 5.2 %convolution_convert_fusion.4 = bf16[512,1536]{1,0:T(8,128)(2,1)} fusion(bf16[1024,1536]{1,0:T(8,128)(2,1)} %param.14, bf16[512,1024]{1,0:T(8,128)(2,1)} %param.11, f32[1024]{0:T(1024)S(1)} %convert_element_type.74, f32[512]{0:T(512)S(1)} %add_rsqrt_fusion.1), kind=kOutput, calls=%fused_computation.10 | convolution fusion | flops 1613496320 | bytes 5773312 | tf_op jit(solution)/shard_map/dot_general | solution.py:17
  35.6 2.6 copy.14
  38.2 0.0 reduce-scatter.21.cloned.1.call-update
  38.2 0.0 reduce-scatter.15.cloned.1.call-start
  38.2 25.8 %reduce-scatter.19.cloned.1.call-done = bf16[384,512]{1,0:T(8,128)(2,1)} async-done(((bf16[1536,512]{1,0:T(8,128)(2,1)}), bf16[384,512]{1,0:T(8,128)(2,1)}) %reduce-scatter.19.cloned.1.call-update) | async-done | bytes 393232
  64.1 1.2 copy.13
  65.3 35.4 %reduce-scatter.21.cloned.1.call-done = bf16[384,512]{1,0:T(8,128)(2,1)} async-done(((bf16[1536,512]{1,0:T(8,128)(2,1)}), bf16[384,512]{1,0:T(8,128)(2,1)}) %reduce-scatter.21.cloned.1.call-update) | async-done | bytes 393232
  100.7 1.9 copy.15
  102.6 0.0 copy-done
  102.6 5.3 %convolution_convert_fusion.1 = bf16[512,4096]{1,0:T(8,128)(2,1)} fusion(bf16[384,4096]{1,0:T(8,128)(2,1)S(1)} %copy-done, bf16[512,384]{1,0:T(8,128)(2,1)} %copy.15, bf16[512,384]{1,0:T(8,128)(2,1)S(1)} %copy.13), kind=kOutput, calls=%fused_computation.1 | convolution fusion | flops 1614282752 | bytes 8126464 | tf_op jit(solution)/shard_map/dot_general | solution.py:27
  107.9 0.0 copy-start.1
  107.9 0.0 copy-start.2
  107.9 0.0 reduce-scatter.15.cloned.1.call-update
  108.0 0.0 all-reduce.3.cloned.1.call-start
  108.0 75.7 %reduce-scatter.15.cloned.1.call-done = bf16[512,1024]{1,0:T(8,128)(2,1)} async-done(((bf16[512,4096]{1,0:T(8,128)(2,1)}), bf16[512,1024]{1,0:T(8,128)(2,1)}) %reduce-scatter.15.cloned.1.call-update) | async-done | bytes 1048592 | tf_op jit(solution)/shard_map/reduce_scatter | solution.py:28
  183.7 0.0 all-reduce.3.cloned.1.call-update
  183.8 0.0 reduce-scatter.23.cloned.1.call-start
  183.8 0.0 copy-done.1
  183.8 0.0 copy-done.2
  183.9 55.8 %all-reduce.3.cloned.1.call-done = bf16[512,1024]{1,0:T(8,128)(2,1)} async-done(((bf16[512,1024]{1,0:T(8,128)(2,1)}), bf16[512,1024]{1,0:T(8,128)(2,1)}) %all-reduce.3.cloned.1.call-update) | async-done | bytes 1048592 | tf_op jit(solution)/shard_map/psum | solution.py:31
  239.7 3.0 fusion.7
  242.7 11.7 %psum.30 = f32[512]{0:T(512)S(1)} all-reduce(f32[512]{0:T(512)S(1)} %get-tuple-element.5), channel_id=1, replica_groups=mesh['ra'=4,'cb'=4,'dp'=2] {'ra'}, use_global_device_ids=true, to_apply=%region_7.8 | all-reduce | flops 512 | bytes 4096 | tf_op jit(solution)/shard_map/psum | solution.py:13
  254.3 5.3 %convolution_convert_fusion.3 = bf16[512,1536]{1,0:T(8,128)(2,1)} fusion(bf16[1024,1536]{1,0:T(8,128)(2,1)} %param.18, bf16[512,1024]{1,0:T(8,128)(2,1)} %get-tuple-element.6, f32[1024]{0:T(1024)S(1)} %convert_element_type.86, f32[512]{0:T(512)S(1)} %add_rsqrt_fusion), kind=kOutput, calls=%fused_computation.9 | convolution fusion | flops 1613496320 | bytes 5773312 | tf_op jit(solution)/shard_map/dot_general | solution.py:16
  259.6 2.6 copy.16
  262.2 0.0 reduce-scatter.23.cloned.1.call-update
  262.2 0.0 reduce-scatter.25.cloned.1.call-start
  262.3 5.3 %convolution_convert_fusion.2 = bf16[512,1536]{1,0:T(8,128)(2,1)} fusion(bf16[1024,1536]{1,0:T(8,128)(2,1)} %param.19, bf16[512,1024]{1,0:T(8,128)(2,1)} %get-tuple-element.6, f32[1024]{0:T(1024)S(1)} %convert_element_type.86, f32[512]{0:T(512)S(1)} %add_rsqrt_fusion), kind=kOutput, calls=%fused_computation.8 | convolution fusion | flops 1613496320 | bytes 5773312 | tf_op jit(solution)/shard_map/dot_general | solution.py:17
  267.5 2.6 copy.18
  270.1 0.0 reduce-scatter.25.cloned.1.call-update
  270.2 0.2 reduce-scatter.17.cloned.1.call-start
  270.4 24.7 %reduce-scatter.23.cloned.1.call-done = bf16[384,512]{1,0:T(8,128)(2,1)} async-done(((bf16[1536,512]{1,0:T(8,128)(2,1)}), bf16[384,512]{1,0:T(8,128)(2,1)}) %reduce-scatter.23.cloned.1.call-update) | async-done | bytes 393232
  295.1 1.2 copy.17
  296.3 35.3 %reduce-scatter.25.cloned.1.call-done = bf16[384,512]{1,0:T(8,128)(2,1)} async-done(((bf16[1536,512]{1,0:T(8,128)(2,1)}), bf16[384,512]{1,0:T(8,128)(2,1)}) %reduce-scatter.25.cloned.1.call-update) | async-done | bytes 393232
  331.5 1.9 copy.19
  333.4 6.3 %convolution_convert_fusion = bf16[512,4096]{1,0:T(8,128)(2,1)} fusion(bf16[384,4096]{1,0:T(8,128)(2,1)} %param.20, bf16[512,384]{1,0:T(8,128)(2,1)} %copy.19, bf16[512,384]{1,0:T(8,128)(2,1)S(1)} %copy.17), kind=kOutput, calls=%fused_computation | convolution fusion | flops 1614282752 | bytes 8126464 | tf_op jit(solution)/shard_map/dot_general | solution.py:27
  339.8 0.0 copy-start.3
  339.8 0.0 reduce-scatter.17.cloned.1.call-update
  339.8 0.0 all-reduce.5.cloned.1.call-start
  339.9 75.8 %reduce-scatter.17.cloned.1.call-done = bf16[512,1024]{1,0:T(8,128)(2,1)} async-done(((bf16[512,4096]{1,0:T(8,128)(2,1)}), bf16[512,1024]{1,0:T(8,128)(2,1)}) %reduce-scatter.17.cloned.1.call-update) | async-done | bytes 1048592 | tf_op jit(solution)/shard_map/reduce_scatter | solution.py:28
  415.6 0.0 all-reduce.5.cloned.1.call-update
  415.6 0.0 copy-done.3
  415.7 56.0 %all-reduce.5.cloned.1.call-done = bf16[512,1024]{1,0:T(8,128)(2,1)} async-done(((bf16[512,1024]{1,0:T(8,128)(2,1)}), bf16[512,1024]{1,0:T(8,128)(2,1)}) %all-reduce.5.cloned.1.call-update) | async-done | bytes 1048592 | tf_op jit(solution)/shard_map/psum | solution.py:31
  471.7 3.0 fusion.6
  (5 shorter events, 0.0 us)
Async XLA Ops:
  6.5 96.1 %copy-start = (bf16[384,4096]{1,0:T(8,128)(2,1)S(1)}, bf16[384,4096]{1,0:T(8,128)(2,1)}, u32[]{:S(2)}) copy-start(bf16[384,4096]{1,0:T(8,128)(2,1)} %param.15) | copy-start | bytes 9437188
  6.5 57.5 %reduce-scatter.19.cloned.1.call-start = ((), (), s32[]{:S(2)}) async-start(), calls=%async_computation.10 | async-start | bytes 1966080
  30.3 70.4 %reduce-scatter.21.cloned.1.call-start = ((), (), s32[]{:S(2)}) async-start(), calls=%async_computation.11 | async-start | bytes 1966080
  38.2 145.6 %reduce-scatter.15.cloned.1.call-start = ((), (), s32[]{:S(2)}) async-start(), calls=%async_computation.6 | async-start | bytes 5242880 | tf_op jit(solution)/shard_map/reduce_scatter | solution.py:28
  107.9 75.9 %copy-start.1 = (bf16[1024]{0:T(1024)(128)(2,1)S(1)}, bf16[1024]{0:T(1024)(128)(2,1)}, u32[]{:S(2)}) copy-start(bf16[1024]{0:T(1024)(128)(2,1)} %param.17) | copy-start | bytes 6148
  107.9 75.9 %copy-start.2 = (bf16[1024]{0:T(1024)(128)(2,1)S(1)}, bf16[1024]{0:T(1024)(128)(2,1)}, u32[]{:S(2)}) copy-start(bf16[1024]{0:T(1024)(128)(2,1)} %param.16) | copy-start | bytes 6148
  108.0 131.7 %all-reduce.3.cloned.1.call-start = ((), (), s32[]{:S(2)}) async-start(), calls=%async_computation.7 | async-start | bytes 2097152 | tf_op jit(solution)/shard_map/psum | solution.py:31
  183.8 111.3 %reduce-scatter.23.cloned.1.call-start = ((), (), s32[]{:S(2)}) async-start(), calls=%async_computation.12 | async-start | bytes 1966080
  262.2 69.3 %reduce-scatter.25.cloned.1.call-start = ((), (), s32[]{:S(2)}) async-start(), calls=%async_computation.13 | async-start | bytes 1966080
  270.2 145.5 %reduce-scatter.17.cloned.1.call-start = ((), (), s32[]{:S(2)}) async-start(), calls=%async_computation.8 | async-start | bytes 5242880 | tf_op jit(solution)/shard_map/reduce_scatter | solution.py:28
  339.8 75.9 %copy-start.3 = (bf16[1024]{0:T(1024)(128)(2,1)S(1)}, bf16[1024]{0:T(1024)(128)(2,1)}, u32[]{:S(2)}) copy-start(bf16[1024]{0:T(1024)(128)(2,1)} %param.21) | copy-start | bytes 6148
  339.8 131.9 %all-reduce.5.cloned.1.call-start = ((), (), s32[]{:S(2)}) async-start(), calls=%async_computation.9 | async-start | bytes 2097152 | tf_op jit(solution)/shard_map/psum | solution.py:31
Sparse Core Ops, SparseCore 0:
  30.4 33.6 reduce-scatter.18
  66.4 34.2 reduce-scatter.20
  108.1 75.6 reduce-scatter.14
  186.7 52.9 all-reduce.2
  262.4 32.6 reduce-scatter.22
  297.2 34.2 reduce-scatter.24
  339.9 75.6 reduce-scatter.16
  418.7 52.9 all-reduce.4
where the time goes:
time: 482 us; the launch traced here: 481 us
  waiting for transfers between devices  385 us (80%)
  matrix products  32.7 us (7%)
  blocking collectives  25.1 us (5%)
  local copies, waits for them, and re-layouts  16.7 us (3%)
  between operations  13.6 us (3%)
  other arithmetic  8.34 us (2%)
    reduce_scatter x2, waiting for transfers between devices, half_step(): lax.psum_scatter(terms.astype(jnp.bfloat16), 'ra', scatter_dimension=1, t...  151 us
    unnamed x12, waiting for transfers between devices  121 us
    psum x2, waiting for transfers between devices, half_step(): branch = lax.psum(partial_value, 'cb').astype(jnp.float32)  112 us
    psum x2, blocking collectives, half_step(): squares = lax.psum(jnp.sum(wide_values * wide_values, axis=1), 'ra')  25.1 us
    unnamed x16, local copies, waits for them, and re-layouts  16.7 us
    dot_general x2, matrix products, half_step(): terms = jnp.dot(hidden, w_down, preferred_element_type=jnp.float32)  11.7 us
    dot_general x2, matrix products, half_step(): gate_part = jnp.dot(normed, w_gate, preferred_element_type=jnp.float32)  10.5 us
    dot_general x2, matrix products, half_step(): up_part = jnp.dot(normed, w_up, preferred_element_type=jnp.float32)  10.5 us
  transfers between devices with their start and end apart: 8, of which 8 were waited for; matrix products, arithmetic and copies ran while one was open for 4% of the time, Pallas kernels for 0%

commit v1 on v0

--- a/solution.py
+++ b/solution.py
@@ -1,10 +1,16 @@
+import functools
+
 import jax
 import jax.numpy as jnp
 from jax import lax
+from jax.experimental import pallas as pl
+from jax.experimental.pallas import tpu as pltpu
 from jax.sharding import PartitionSpec as P
 
 epsilon = 1e-06
 residual_scale = 0.25
+MESH = pl.DeviceIdType.MESH
+CHUNKS = 4
 
 
 def half_step(values, norm_gain, w_gate, w_up, w_down, branch_gain):
@@ -34,7 +40,7 @@
     )
 
 
-def shards(
+def plain(
     tokens,
     first_gain,
     first_gate,
@@ -49,6 +55,438 @@
 ):
     middle = half_step(tokens, first_gain, first_gate, first_up, first_down, first_branch)
     return half_step(middle, second_gain, second_gate, second_up, second_down, second_branch)
+
+
+def kernel(
+    n, m, K, rows, wide, hid,
+    tok, gate0, up0, down0, gate1, up1, down1, gains, branches, out,
+    wgu, wd, xbuf, xg, part, recv_a, yst, recv_y, sst, recv_s, acc, ytot, ownz, sq, recv_q,
+    w_sem, d_sem, x_sem, o_sem,
+    as_sem, ar_sem, ys_sem, yr_sem, ss_sem, sr_sem, gs_sem, gr_sem, qs_sem, qr_sem,
+):
+    r = lax.axis_index("ra")
+    c = lax.axis_index("cb")
+    T = rows // K
+    q = wide // m
+    full = n * wide
+    S = 2 * K
+    f32 = jnp.float32
+
+    def w_copies(h):
+        gate, up = ((gate0, up0), (gate1, up1))[h]
+        made = []
+        for d in range(n):
+            for i, src in enumerate((gate, up)):
+                made.append(pltpu.make_async_copy(
+                    src.at[:, pl.ds(d * hid, hid)],
+                    wgu.at[h, d, :, pl.ds(i * hid, hid)],
+                    w_sem.at[h, d, i],
+                ))
+        return made
+
+    def d_copies(h):
+        down = (down0, down1)[h]
+        return [
+            pltpu.make_async_copy(
+                down.at[:, pl.ds(z * wide + p * q, q)],
+                wd.at[h, p, :, pl.ds(z * q, q)],
+                d_sem.at[h, p, z],
+            )
+            for p in range(m)
+            for z in range(n)
+        ]
+
+    x_copies = [
+        pltpu.make_async_copy(tok.at[:, pl.ds(p * q, q)], xbuf.at[0, p], x_sem.at[p])
+        for p in range(m)
+    ]
+    for copy in x_copies + w_copies(0) + d_copies(0) + w_copies(1) + d_copies(1):
+        copy.start()
+
+    barrier = pltpu.get_barrier_semaphore()
+    for o in range(1, n):
+        pl.semaphore_signal(barrier, inc=1, device_id={"ra": lax.rem(r + o, n)}, device_id_type=MESH)
+    for o in range(1, m):
+        pl.semaphore_signal(barrier, inc=1, device_id={"cb": lax.rem(c + o, m)}, device_id_type=MESH)
+
+    def rows_of(k):
+        return pl.ds(pl.multiple_of(k * T, T), T)
+
+    def a_copy(s, d, target, slot):
+        h, k = s // K, s % K
+        return pltpu.make_async_remote_copy(
+            src_ref=part.at[d, rows_of(k)],
+            dst_ref=recv_a.at[h, slot, rows_of(k)],
+            send_sem=as_sem.at[k, d],
+            recv_sem=ar_sem.at[s, slot],
+            device_id={"ra": target},
+            device_id_type=MESH,
+        )
+
+    def y_copy(s, dest, src):
+        h, k = s // K, s % K
+        return pltpu.make_async_remote_copy(
+            src_ref=yst.at[dest, rows_of(k)],
+            dst_ref=recv_y.at[h, src, rows_of(k)],
+            send_sem=ys_sem.at[k, dest],
+            recv_sem=yr_sem.at[s, src],
+            device_id={"cb": dest},
+            device_id_type=MESH,
+        )
+
+    def s_copy(s, dest, src):
+        h, k = s // K, s % K
+        return pltpu.make_async_remote_copy(
+            src_ref=sst.at[dest, rows_of(k)],
+            dst_ref=recv_s.at[h, src, rows_of(k)],
+            send_sem=ss_sem.at[k, dest],
+            recv_sem=sr_sem.at[s, src],
+            device_id={"ra": dest},
+            device_id_type=MESH,
+        )
+
+    def g_copy(s, dest, src):
+        h, k = s // K, s % K
+        return pltpu.make_async_remote_copy(
+            src_ref=xbuf.at[h + 1, src, rows_of(k)],
+            dst_ref=xbuf.at[h + 1, src, rows_of(k)],
+            send_sem=gs_sem.at[s, dest],
+            recv_sem=gr_sem.at[s, src],
+            device_id={"cb": dest},
+            device_id_type=MESH,
+        )
+
+    def q_copy(s, dest, src):
+        return pltpu.make_async_remote_copy(
+            src_ref=sq.at[s],
+            dst_ref=recv_q.at[s, src],
+            send_sem=qs_sem.at[s, dest],
+            recv_sem=qr_sem.at[s, src],
+            device_id={"ra": dest},
+            device_id_type=MESH,
+        )
+
+    def send_part(s, d, value, target, slot):
+        k = s % K
+
+        @pl.when(s >= K)
+        def _():
+            a_copy(s, d, target, slot).wait_send()
+
+        part[d, rows_of(k), :] = value.astype(jnp.bfloat16)
+        a_copy(s, d, target, slot).start()
+
+    def ahead(s):
+        h, k = s // K, s % K
+        total = jnp.zeros((T, 128), f32)
+        for p in range(m):
+            x = xbuf[h, p, rows_of(k), :].astype(f32)
+            xg[rows_of(k), p * q:(p + 1) * q] = (x * gains[h, :, p * q:(p + 1) * q]).astype(jnp.bfloat16)
+            x2 = x * x
+            for i in range(q // 128):
+                total = total + x2[:, i * 128:(i + 1) * 128]
+        column = jnp.sum(total, axis=1, keepdims=True)
+        sq[s] = jnp.transpose(jnp.broadcast_to(column, (T, 128)))[:8]
+
+        def q_send(o, carry):
+            q_copy(s, lax.rem(r + o, n), r).start()
+            return carry
+
+        lax.fori_loop(1, n, q_send, 0)
+
+        @pl.when(jnp.logical_or(r == 0, r == n - 1))
+        def _():
+            def head(j, carry):
+                d = jnp.where(r == 0, n - 1 - j, j)
+                target = jnp.where(r == 0, 1, n - 2)
+                slot = jnp.where(r == 0, d + 1, d)
+                value = jnp.dot(xg[rows_of(k), :], wgu[h, d], preferred_element_type=f32)
+                send_part(s, d, value, target, slot)
+                return carry
+
+            lax.fori_loop(0, n - 1, head, 0)
+
+    def forward(s, leftward):
+        h, k = s // K, s % K
+
+        def step(j, carry):
+            d = jnp.where(leftward, j, n - 1 - j)
+            target = jnp.where(leftward, r - 1, r + 1)
+            slot = jnp.where(leftward, d, d + 1)
+
+            @pl.when(jnp.where(leftward, d < r, d > r))
+            def _():
+                acc[...] = jnp.dot(xg[rows_of(k), :], wgu[h, d], preferred_element_type=f32)
+                a_copy(s, d, target, slot).wait_recv()
+                send_part(s, d, acc[...] + recv_a[h, slot, rows_of(k), :].astype(f32), target, slot)
+
+            return carry
+
+        @pl.when(jnp.logical_and(r > 0, r < n - 1))
+        def _():
+            lax.fori_loop(0, n - 1, step, 0)
+
+    near_left = r >= n // 2
+    far_left = r < n // 2
+
+    def finish(s):
+        h, k = s // K, s % K
+        acc[...] = jnp.dot(xg[rows_of(k), :], wgu[h, r], preferred_element_type=f32)
+
+        def q_wait(o, carry):
+            src = lax.rem(r + o, n)
+            q_copy(s, src, src).wait_recv()
+            return carry + recv_q[s, src]
+
+        squares = lax.fori_loop(1, n, q_wait, sq[s])
+        scale_row = lax.rsqrt(squares / full + epsilon)
+        scale = jnp.transpose(jnp.broadcast_to(scale_row[:1], (128, T)))[:, :1]
+
+        @pl.when(r > 0)
+        def _():
+            a_copy(s, r, r, r + 1).wait_recv()
+            acc[...] += recv_a[h, r + 1, rows_of(k), :].astype(f32)
+
+        @pl.when(r < n - 1)
+        def _():
+            a_copy(s, r, r, r).wait_recv()
+            acc[...] += recv_a[h, r, rows_of(k), :].astype(f32)
+
+        gate = acc[:, :hid] * scale
+        upward = acc[:, hid:] * scale
+        hidden = (gate / (1.0 + jnp.exp(-gate)) * upward).astype(jnp.bfloat16)
+
+        def down(o, carry):
+            dest = lax.rem(c + o, m)
+            value = jnp.dot(hidden, wd[h, dest], preferred_element_type=f32)
+
+            @pl.when(s >= K)
+            def _():
+                y_copy(s, dest, c).wait_send()
+
+            yst[dest, rows_of(k), :] = value.astype(jnp.bfloat16)
+            y_copy(s, dest, c).start()
+            return carry
+
+        lax.fori_loop(1, m, down, 0)
+        ytot[...] = jnp.dot(hidden, wd[h, c], preferred_element_type=f32)
+
+    def plane(s):
+        h, k = s // K, s % K
+
+        def add(o, carry):
+            src = lax.rem(c + o, m)
+            y_copy(s, src, src).wait_recv()
+            ytot[...] += recv_y[h, src, rows_of(k), :].astype(f32)
+            return carry
+
+        lax.fori_loop(1, m, add, 0)
+
+        def send(o, carry):
+            dest = lax.rem(r + o, n)
+
+            @pl.when(s >= K)
+            def _():
+                s_copy(s, dest, r).wait_send()
+
+            sst[dest, rows_of(k), :] = ytot[:, pl.ds(pl.multiple_of(dest * q, q), q)].astype(jnp.bfloat16)
+            s_copy(s, dest, r).start()
+            return carry
+
+        lax.fori_loop(1, n, send, 0)
+        ownz[rows_of(k), :] = ytot[:, pl.ds(pl.multiple_of(r * q, q), q)]
+
+    def gather(s):
+        h, k = s // K, s % K
+
+        def add(o, carry):
+            src = lax.rem(r + o, n)
+            s_copy(s, src, src).wait_recv()
+            ownz[rows_of(k), :] += recv_s[h, src, rows_of(k), :].astype(f32)
+            return carry
+
+        lax.fori_loop(1, n, add, 0)
+        gain = branches[h, :, pl.ds(pl.multiple_of(c * q, q), q)]
+        x = xbuf[h, c, rows_of(k), :].astype(f32)
+        xbuf[h + 1, c, rows_of(k), :] = (
+            residual_scale * x + 0.5 * gain * ownz[rows_of(k), :]
+        ).astype(jnp.bfloat16)
+
+        def send(o, carry):
+            g_copy(s, lax.rem(c + o, m), c).start()
+            return carry
+
+        lax.fori_loop(1, m, send, 0)
+
+    def o_copy(k, p):
+        return pltpu.make_async_copy(
+            xbuf.at[2, p, rows_of(k)], out.at[rows_of(k), pl.ds(p * q, q)], o_sem.at[k, p]
+        )
+
+    def arrive(s):
+        k = s % K
+
+        def wait(o, carry):
+            src = lax.rem(c + o, m)
+            g_copy(s, src, src).wait_recv()
+            return carry
+
+        lax.fori_loop(1, m, wait, 0)
+
+        @pl.when(s >= K)
+        def _():
+            for p in range(m):
+                o_copy(k, p).start()
+
+    for copy in x_copies + w_copies(0):
+        copy.wait()
+    pl.semaphore_wait(barrier, n + m - 2)
+    ahead(jnp.int32(0))
+    forward(jnp.int32(0), near_left)
+    for copy in d_copies(0):
+        copy.wait()
+
+    def slot_body(t, carry):
+        @pl.when(t == K - 1)
+        def _():
+            for copy in w_copies(1) + d_copies(1):
+                copy.wait()
+
+        @pl.when(jnp.logical_and(t >= 3, t < S + 3))
+        def _():
+            arrive(t - 3)
+
+        @pl.when(t + 1 < S)
+        def _():
+            ahead(t + 1)
+
+        @pl.when(t < S)
+        def _():
+            forward(t, far_left)
+
+        @pl.when(jnp.logical_and(t >= 2, t < S + 2))
+        def _():
+            gather(t - 2)
+
+        @pl.when(jnp.logical_and(t >= 1, t < S + 1))
+        def _():
+            plane(t - 1)
+
+        @pl.when(t < S)
+        def _():
+            finish(t)
+
+        @pl.when(t + 1 < S)
+        def _():
+            forward(t + 1, near_left)
+
+        return carry
+
+    lax.fori_loop(0, S + 3, slot_body, 0)
+
+    def drain(k, carry):
+        def over_ra(o, inner):
+            dest = lax.rem(r + o, n)
+            a_copy(k, dest, dest, dest).wait_send()
+            s_copy(k, dest, r).wait_send()
+            q_copy(k, dest, r).wait_send()
+            q_copy(k + K, dest, r).wait_send()
+            return inner
+
+        def over_cb(o, inner):
+            dest = lax.rem(c + o, m)
+            y_copy(k, dest, c).wait_send()
+            g_copy(k, dest, c).wait_send()
+            g_copy(k + K, dest, c).wait_send()
+            return inner
+
+        lax.fori_loop(1, n, over_ra, 0)
+        lax.fori_loop(1, m, over_cb, 0)
+        for p in range(m):
+            o_copy(k, p).wait()
+        return carry
+
+    lax.fori_loop(0, K, drain, 0)
+
+
+def fused(
+    tokens,
+    first_gain,
+    first_gate,
+    first_up,
+    first_down,
+    first_branch,
+    second_gain,
+    second_gate,
+    second_up,
+    second_down,
+    second_branch,
+):
+    n, m = lax.axis_size("ra"), lax.axis_size("cb")
+    rows, wide = tokens.shape
+    hid = first_down.shape[0]
+    K = CHUNKS
+    S = 2 * K
+    T = rows // K
+    q = wide // m
+    f32, bf16 = jnp.float32, jnp.bfloat16
+    gains = jnp.stack([first_gain, second_gain]).astype(f32).reshape(2, 1, wide)
+    branches = jnp.stack([first_branch, second_branch]).astype(f32).reshape(2, 1, wide)
+    dma = pltpu.SemaphoreType.DMA
+    anywhere = pl.BlockSpec(memory_space=pl.ANY)
+    inside = pl.BlockSpec(memory_space=pltpu.VMEM)
+    return pl.pallas_call(
+        functools.partial(kernel, n, m, K, rows, wide, hid),
+        out_shape=jax.ShapeDtypeStruct((rows, wide), bf16),
+        in_specs=[anywhere] * 7 + [inside] * 2,
+        out_specs=anywhere,
+        scratch_shapes=[
+            pltpu.VMEM((2, n, wide, 2 * hid), bf16),
+            pltpu.VMEM((2, m, hid, n * q), bf16),
+            pltpu.VMEM((3, m, rows, q), bf16),
+            pltpu.VMEM((rows, wide), bf16),
+            pltpu.VMEM((n, rows, 2 * hid), bf16),
+            pltpu.VMEM((2, n + 1, rows, 2 * hid), bf16),
+            pltpu.VMEM((m, rows, n * q), bf16),
+            pltpu.VMEM((2, m, rows, n * q), bf16),
+            pltpu.VMEM((n, rows, q), bf16),
+            pltpu.VMEM((2, n, rows, q), bf16),
+            pltpu.VMEM((T, 2 * hid), f32),
+            pltpu.VMEM((T, n * q), f32),
+            pltpu.VMEM((rows, q), f32),
+            pltpu.VMEM((S, 8, T), f32),
+            pltpu.VMEM((S, n, 8, T), f32),
+            dma((2, n, 2)),
+            dma((2, m, n)),
+            dma((m,)),
+            dma((K, m)),
+            dma((K, n)),
+            dma((S, n + 1)),
+            dma((K, m)),
+            dma((S, m)),
+            dma((K, n)),
+            dma((S, n)),
+            dma((S, m)),
+            dma((S, m)),
+            dma((S, n)),
+            dma((S, n)),
+        ],
+        compiler_params=pltpu.CompilerParams(
+            collective_id=0, has_side_effects=True, vmem_limit_bytes=66000000
+        ),
+        name="ffn_pair",
+    )(
+        tokens, first_gate, first_up, first_down, second_gate, second_up, second_down,
+        gains, branches,
+    )
+
+
+def shards(*arrays):
+    n, m = lax.axis_size("ra"), lax.axis_size("cb")
+    rows, wide = arrays[0].shape
+    hid = arrays[4].shape[0]
+    even = rows % (128 * CHUNKS) == 0 and hid % 128 == 0 and wide % (128 * m) == 0
+    return fused(*arrays) if even and n > 1 and m > 1 else plain(*arrays)
 
 
 def solution(mesh):

time: 482 us -> 178 us (0.37)
  waiting for transfers between devices: 385 us -> 0 us
  Pallas kernels: 0 us -> 172 us
  matrix products: 32.7 us -> 0 us
  blocking collectives: 25.1 us -> 0 us
  between operations: 13.6 us -> 0.01 us
  local copies, waits for them, and re-layouts: 16.7 us -> 5 us
  other arithmetic: 8.34 us -> 0.62 us
    pallas_call x0 -> x1, Pallas kernels: none -> 172 us  [fused(): pl.pallas_call(functools.partial(kernel, n, m, K, rows, wide, hid), out_s...]
    reduce_scatter x2 -> x0, waiting for transfers between devices: 151 us -> none  [half_step(): lax.psum_scatter(terms.astype(jnp.bfloat16), 'ra', scatter_dimension=1, t...]
    unnamed x12 -> x0, waiting for transfers between devices: 121 us -> none
    psum x2 -> x0, waiting for transfers between devices: 112 us -> none  [half_step(): branch = lax.psum(partial_value, 'cb').astype(jnp.float32)]
    dot_general x6 -> x0, matrix products: 32.7 us -> none  [the longest x2 11.7 us: half_step(): terms = jnp.dot(hidden, w_down, preferred_element_type=jnp.float32)]
    psum x2 -> x0, blocking collectives: 25.1 us -> none  [half_step(): squares = lax.psum(jnp.sum(wide_values * wide_values, axis=1), 'ra')]
    unnamed x16 -> x1, local copies, waits for them, and re-layouts: 16.7 us -> 2.26 us
  transfers between devices with their start and end apart: 8 -> 0, of which waited for: 8 -> 0; matrix products, arithmetic and copies ran while one was open for 4% -> 0% of each run, Pallas kernels for 0% -> 0%
where the time goes in v1:
time: 178 us; the launch traced here: 177 us
  Pallas kernels  172 us (97%)
  local copies, waits for them, and re-layouts  5 us (3%)
    pallas_call x1, Pallas kernels, fused(): pl.pallas_call(functools.partial(kernel, n, m, K, rows, wide, hid), out_s...  172 us

profile of v1, /device:TPU:0, one launch (start us, length us, event | category | flops | bytes accessed | tf_op | source)
XLA Modules:
  0.0 177.4 jit_solution(13634314318477097480)
XLA Ops:
  0.0 0.7 stack.18
  0.7 0.7 stack.21
  1.4 0.7 stack.19
  2.1 0.7 stack.22
  2.7 0.6 maximum_convert_fusion
  3.4 171.7 %ffn_pair.1 = bf16[512,1024]{1,0:T(8,128)(2,1)} custom-call(bf16[512,1024]{1,0:T(8,128)(2,1)} %tok.1, bf16[1024,1536]{1,0:T(8,128)(2,1)} %gate0.1, bf16[1024,1536]{1,0:T(8,128)(2,1)} %up0.1, bf16[384,4096]{1,0:T(8,128)(2,1)} %down0.1, bf16[1024,1536]{1,0:T(8,128)(2,1)} %gate1.1, bf16[1024,1536]{1,0:T(8,128)(2,1)} %up1.1, bf16[384,4096]{1,0:T(8,128)(2,1)} %down1.1, ...), custom_call_target="tpu_custom_call" | custom-call | tf_op jit(solution)/shard_map/ffn_pair/pallas_call | solution.py:438
  175.1 2.3 %copy.13 = bf16[512,1024]{1,0:T(8,128)(2,1)} copy(bf16[512,1024]{1,0:T(8,128)(2,1)} %ffn_pair.1) | data formatting | bytes 2097152
